TPU v7x, 256 devices: a whole 4x4x8 slice. The times are simulated.
256 devices in a mesh: sp: 16 (over y, x), tp: 16 (over z, core).
Axes of the slice: x: 4, y: 4, z: 8, core: 2. Of those that a mesh axis runs over, the one named last changes fastest.
Arguments:
- tokens: bfloat16 [8192, 2048], P(('sp', 'tp')), may hold values from -6 to 6
- query_vectors: bfloat16 [8192, 2048], P('sp', 'tp'), may hold values from -8 to 8
- key_vectors: bfloat16 [8192, 2048], P('sp', 'tp'), may hold values from -8 to 8
- value_vectors: bfloat16 [8192, 2048], P('sp', 'tp'), may hold values from -24 to 24
- cum_gate: float32 [8192, 32], P('sp', 'tp'), may hold values from -1028 to 0, as said below
- out_weight: bfloat16 [2048, 2048], P('tp'), may hold values from -0.125 to 0.125
- norm_gain: float32 [2048], replicated, may hold values from 0.1 to 1.9
- gate_weight: bfloat16 [16, 2048, 7168], P('sp', None, 'tp'), may hold values from -0.125 to 0.125
- up_weight: bfloat16 [16, 2048, 7168], P('sp', None, 'tp'), may hold values from -0.125 to 0.125
- down_weight: bfloat16 [16, 7168, 2048], P('sp', 'tp'), may hold values from -0.0625 to 0.0625
- expert_ids: int32 [8192, 2], P(('sp', 'tp')), may hold values from 0 to 15, all different within a row; in each aligned block of 32 rows (0 to 31, 32 to 63, ...) at most 6 rows name the same one
- route_weights: float32 [8192, 2], P(('sp', 'tp')), may hold values from 0.2 to 1
Outputs:
- layer_output: bfloat16 [8192, 2048], P(('sp', 'tp'))
Inputs may be any that keep to these rules, and one draw needn't show every extreme that they name: `cum_gate`: along the positions each head's values never rise. `expert_ids`: within the rows of one device no expert is named by more than 6 rows, and in some devices' rows one expert is named by exactly 6; a row names 2 different experts.
All inputs are finite; a program needn't handle non-finite values.
Results may differ from a plain program's by a relative error of at most 0.014.
Values may be sent and summed in bfloat16 or wider, within the bound.
A program may use at most 128 MiB of HBM per device.

v0:
```python
import math
import jax
import jax.numpy as jnp
from jax import lax
from jax.sharding import PartitionSpec as P

NEG_LARGE = -1e30


def copy_for_each(shard, axis):
    peers = lax.axis_size(axis)
    return lax.all_to_all(
        jnp.broadcast_to(shard[None], (peers, *shard.shape)), axis, 0, 0, tiled=True
    )


def in_order(parts, dim):
    parts = jnp.moveaxis(parts, 0, dim)
    dims = parts.shape
    return parts.reshape(*dims[:dim], dims[dim] * dims[dim + 1], *dims[dim + 2 :])


def collect(shard, axis, dim):
    parts = copy_for_each(shard, axis)
    return in_order(parts, dim)


def sent_together(arrays, axis, dim, along):
    widths = [a.shape[along] for a in arrays]
    both = jnp.concatenate(arrays, axis=along)
    filled = lax.all_gather(both, axis, axis=dim, tiled=True)
    return tuple(jnp.split(filled, [sum(widths[:k]) for k in range(1, len(widths))], axis=along))


def shards(
    tokens,
    query_vectors,
    key_vectors,
    value_vectors,
    cum_gate,
    out_weight,
    norm_gain,
    gate_weight,
    up_weight,
    down_weight,
    expert_ids,
    route_weights,
):
    sp_count = lax.axis_size("sp")
    seg_rows = query_vectors.shape[0]
    heads_here = cum_gate.shape[1]
    head_width = query_vectors.shape[1] // heads_here
    score_scale = head_width ** (-0.5)
    offset = lax.axis_index("sp") * seg_rows
    last_query = offset + seg_rows - 1
    query_pos = offset + jnp.arange(seg_rows, dtype=jnp.int32)
    query_heads = query_vectors.reshape(seg_rows, heads_here, head_width)
    query_gate = cum_gate.T
    gate_rows = collect(cum_gate, "sp", 0)

    def attend_block(carried, key_block, value_block, block_start):
        running_peak, running_total, accumulated = carried
        row_count = key_block.shape[0]
        key_heads = key_block.reshape(row_count, heads_here, head_width)
        value_heads = value_block.reshape(row_count, heads_here, head_width)
        key_gate = lax.dynamic_slice_in_dim(gate_rows, block_start, row_count, 0).T
        scores = (
            jnp.einsum("qhd,khd->hqk", query_heads, key_heads, preferred_element_type=jnp.float32)
            * score_scale
        )
        scores = scores + query_gate[:, :, None] - key_gate[:, None, :]
        key_pos = block_start + jnp.arange(row_count, dtype=jnp.int32)
        visible = (key_pos[None, :] <= query_pos[:, None])[None]
        scores = jnp.where(visible, scores, NEG_LARGE)
        new_peak = jnp.maximum(running_peak, jnp.max(scores, axis=2))
        exponent = jnp.where(visible, jnp.exp(scores - new_peak[:, :, None]), 0.0)
        rescale = jnp.exp(running_peak - new_peak)
        running_total = running_total * rescale + jnp.sum(exponent, axis=2)
        weighted = jnp.einsum(
            "hqk,khd->hqd",
            exponent.astype(jnp.bfloat16),
            value_heads,
            preferred_element_type=jnp.float32,
        )
        accumulated = accumulated * rescale[:, :, None] + weighted
        return (new_peak, running_total, accumulated)

    start_state = (
        jnp.full((heads_here, seg_rows), NEG_LARGE, jnp.float32),
        jnp.zeros((heads_here, seg_rows), jnp.float32),
        jnp.zeros((heads_here, seg_rows, head_width), jnp.float32),
    )
    carried = start_state
    key_piece, value_piece = sent_together((key_vectors, value_vectors), "sp", 0, 1)
    row_count = key_piece.shape[0]
    block_rows = math.gcd(row_count, 1024)
    block_count = row_count // block_rows
    key_stack = key_piece.reshape(block_count, block_rows, key_piece.shape[1])
    value_stack = value_piece.reshape(block_count, block_rows, value_piece.shape[1])

    def step_block(state, inputs):
        key_block, value_block, block_index = inputs
        block_start = block_index * block_rows

        def take_block(inner):
            return attend_block(inner, key_block, value_block, block_start)

        def skip_block(inner):
            return inner

        return (lax.cond(block_start <= last_query, take_block, skip_block, state), None)

    carried, _ = lax.scan(
        step_block, carried, (key_stack, value_stack, jnp.arange(block_count, dtype=jnp.int32))
    )
    final_peak, final_total, accumulated = carried
    attended = (accumulated / final_total[:, :, None]).astype(jnp.bfloat16)
    attended = attended.transpose(1, 0, 2).reshape(seg_rows, heads_here * head_width)
    tok_dev = tokens.shape[0]
    model_width = tokens.shape[1]
    token_rows = lax.all_to_all(attended, "tp", split_axis=0, concat_axis=1, tiled=True)
    projected = jnp.dot(
        token_rows,
        lax.all_gather(out_weight, "tp", axis=0, tiled=True),
        preferred_element_type=jnp.float32,
    )
    stream_wide = (tokens.astype(jnp.float32) + projected).astype(jnp.bfloat16).astype(jnp.float32)
    inverse = lax.rsqrt(jnp.mean(stream_wide * stream_wide, axis=1, keepdims=True) + 1e-05)
    normed = (stream_wide * inverse * norm_gain[None, :]).astype(jnp.bfloat16)
    n_experts = gate_weight.shape[0] * sp_count
    top_count = expert_ids.shape[1]
    capacity = max(2, 3 * tok_dev * top_count // (2 * n_experts))
    flat_ids = expert_ids.reshape(-1)
    hits = (flat_ids[:, None] == jnp.arange(n_experts, dtype=jnp.int32)[None, :]).astype(jnp.int32)
    earlier = jnp.cumsum(hits, axis=0) - hits
    slot_index = flat_ids * capacity + jnp.sum(earlier * hits, axis=1)
    placement_map = (
        jnp.arange(n_experts * capacity, dtype=jnp.int32)[:, None] == slot_index[None, :]
    ).astype(jnp.bfloat16)
    repeated = jnp.repeat(normed, top_count, axis=0)
    dispatch = jnp.dot(placement_map, repeated, preferred_element_type=jnp.float32).astype(
        jnp.bfloat16
    )
    dispatch = dispatch.reshape(n_experts, capacity, model_width)
    arrived = lax.all_to_all(dispatch, "sp", split_axis=0, concat_axis=0, tiled=True)
    row_block = arrived.reshape(-1, model_width)
    rows_in = lax.all_gather(row_block, "tp", axis=0, tiled=True)
    gate_value = jnp.dot(rows_in, gate_weight[0], preferred_element_type=jnp.float32)
    up_value = jnp.dot(rows_in, up_weight[0], preferred_element_type=jnp.float32)
    hidden = (jax.nn.silu(gate_value) * up_value).astype(jnp.bfloat16)
    summed = lax.psum_scatter(
        jnp.dot(hidden, down_weight[0], preferred_element_type=jnp.float32).astype(jnp.bfloat16),
        "tp",
        scatter_dimension=0,
        tiled=True,
    )
    returned = summed.reshape(arrived.shape)
    back = lax.all_to_all(returned, "sp", split_axis=0, concat_axis=0, tiled=True)
    flat_back = back.reshape(n_experts * capacity, model_width)
    picked = flat_back[slot_index].astype(jnp.float32).reshape(tok_dev, top_count, model_width)
    mixture = jnp.sum(picked * route_weights[:, :, None], axis=1)
    return (stream_wide + mixture).astype(jnp.bfloat16)


def solution(mesh):
    in_specs = (
        P(("sp", "tp"), None),
        P("sp", "tp"),
        P("sp", "tp"),
        P("sp", "tp"),
        P("sp", "tp"),
        P("tp", None),
        P(),
        P("sp", None, "tp"),
        P("sp", None, "tp"),
        P("sp", "tp", None),
        P(("sp", "tp"), None),
        P(("sp", "tp"), None),
    )
    out_specs = P(("sp", "tp"), None)
    return jax.shard_map(shards, mesh=mesh, in_specs=in_specs, out_specs=out_specs, check_vma=False)
```

profile of v0, /device:TPU:2, one launch (start us, length us, event | category | flops | bytes accessed | tf_op | source)
XLA Modules:
  0.0 335.4 jit_solution(8175806650671181984)
XLA Ops:
  6.5 1.8 pad_maximum_fusion
  8.4 0.7 all-gather.6.cloned.1.call-update
  9.2 1.3 broadcast_in_dim.61
  10.5 7.5 %all-to-all-start = ((f32[16,512,2]{1,2,0:T(2,128)}), f32[16,512,2]{1,2,0:T(2,128)S(1)}, u32[]{:S(2)}, u32[]{:S(2)}) async-start(f32[16,512,2]{1,2,0:T(2,128)} %broadcast_in_dim.61), calls=%async_computation | async-start | bytes 131072 | tf_op jit(solution)/shard_map/all_to_all | solution.py:12
  18.0 1.0 copy.28
  19.0 0.8 copy.33
  20.0 49.1 %all-gather.4.cloned.1.call-done = bf16[8192,256]{1,0:T(8,128)(2,1)} async-done(((bf16[512,256]{1,0:T(8,128)(2,1)}), bf16[8192,256]{1,0:T(8,128)(2,1)}) %all-gather.4.cloned.1.call-update) | async-done | bytes 4194320 | tf_op jit(solution)/shard_map/all_gather | solution.py:31
  69.2 4.4 %fusion.30 = (bf16[8192,128]{1,0:T(8,128)(2,1)}, bf16[8192,128]{1,0:T(8,128)(2,1)}) fusion(bf16[8192,256]{1,0:T(8,128)(2,1)} %all-gather.4.cloned.1.call-done), kind=kLoop, calls=%fused_computation.54 | loop fusion | bytes 8388608 | tf_op jit(solution)/shard_map/split | solution.py:32
  73.6 3.9 %copy.29 = bf16[8,1024,128]{1,2,0:T(8,128)(2,1)} copy(bf16[8,1024,128]{2,1,0:T(8,128)(2,1)} %bitcast.60) | data formatting | bytes 4194304
  77.5 3.9 %copy.30 = bf16[8,1024,128]{1,2,0:T(8,128)(2,1)} copy(bf16[8,1024,128]{2,1,0:T(8,128)(2,1)} %bitcast.59) | data formatting | bytes 4194304
  81.5 16.5 %while.15 = (s32[]{:T(128)}, f32[2,512]{1,0:T(2,128)S(1)}, f32[2,512]{1,0:T(2,128)S(1)}, f32[2,512,64]{1,2,0:T(8,128)S(1)}, s32[8]{0:T(128)S(1)}, /*index=5*/s32...) while((s32[]{:T(128)}, f32[2,512]{1,0:T(2,128)S(1)}, ...), condition=%wide.region_5.6_spmd.clone, body=%wide.region_0.5_spmd.clone.sunk | while | flops 289017344 | bytes 17043828 | solution.py:113
  82.8 6.2 %conditional.3 = ((f32[2,512]{1,0:T(2,128)S(1)}, f32[2,512]{1,0:T(2,128)S(1)}, f32[2,512,64]{1,2,0:T(8,128)S(1)})) conditional(s32[]{:T(128)} %convert_element_type.83, (f32[2,512]{1,0:T(2,128)S(1)}, f32[2,512]{1,0:T(2,128)S(1)}, f32[2,512,64]{1,2,0:T(8,128)S(1)}) %tuple.43, (s32[]{:T(128)}, s32[]{:T(128)}, bf16[8,1024,128]{1,2,0:T(8,128)(2,1)}, ...), branch_computations={%region_1.1_spmd, %region_2.4_spmd} | conditional | flops 289017344 | bytes 17041490 | solution.py:111
  83.3 1.1 constant_dynamic-slice_fusion
  84.3 1.4 fusion.4
  85.7 1.5 fusion.3
  87.2 1.7 fusion.8
  98.2 0.8 all_to_all.24
  99.0 7.1 %all-to-all-start.1 = ((bf16[16,32,128]{2,1,0:T(8,128)(2,1)}), bf16[16,32,128]{2,1,0:T(8,128)(2,1)S(1)}, u32[]{:S(2)}, u32[]{:S(2)}) async-start(bf16[16,32,128]{2,1,0:T(8,128)(2,1)} %all_to_all.24), calls=%async_computation.1 | async-start | bytes 262144 | tf_op jit(solution)/shard_map/all_to_all | solution.py:121
  106.4 10.4 %all-to-all-done.1 = bf16[16,32,128]{2,1,0:T(8,128)(2,1)S(1)} async-done(((bf16[16,32,128]{2,1,0:T(8,128)(2,1)}), bf16[16,32,128]{2,1,0:T(8,128)(2,1)S(1)}, u32[]{:S(2)}, u32[]{:S(2)}) %all-to-all-start.1) | async-done | bytes 131104 | tf_op jit(solution)/shard_map/all_to_all | solution.py:121
  116.8 12.6 %all-gather.6.cloned.1.call-done = bf16[2048,2048]{1,0:T(8,128)(2,1)} async-done(((bf16[128,2048]{1,0:T(8,128)(2,1)}), bf16[2048,2048]{1,0:T(8,128)(2,1)}) %all-gather.6.cloned.1.call-update) | async-done | bytes 8388624 | tf_op jit(solution)/shard_map/all_gather | solution.py:124
  129.4 5.0 %multiply_reduce_fusion.1 = (f32[32]{0:T(128)S(1)}, f32[32,2048]{1,0:T(8,128)S(1)}) fusion(bf16[2048,2048]{1,0:T(8,128)(2,1)} %all-gather.6.cloned.1.call-done, bf16[32,2048]{1,0:T(8,128)(2,1)S(1)} %copy-done.2, bf16[16,32,128]{2,1,0:T(8,128)(2,1)S(1)} %all-to-all-done.1), kind=kOutput, calls=%fused_computation.36 | convolution fusion | flops 268828640 | bytes 8913024 | tf_op jit(solution)/shard_map/dot_general | solution.py:122
  135.2 44.9 %all_to_all.34 = bf16[16,6,2048]{2,1,0:T(8,128)(2,1)S(1)} all-to-all(bf16[16,6,2048]{2,1,0:T(8,128)(2,1)S(1)} %reshape.145), channel_id=1, replica_groups=mesh['sp'=16,'tp'=16] {'sp'}, dimensions={0} | all-to-all | bytes 786432 | tf_op jit(solution)/shard_map/all_to_all | solution.py:145
  180.1 0.9 reshape.146
  181.3 40.0 %all-gather.8.cloned.1.call-done = bf16[1536,2048]{1,0:T(8,128)(2,1)} async-done(((bf16[96,2048]{1,0:T(8,128)(2,1)}), bf16[1536,2048]{1,0:T(8,128)(2,1)}) %all-gather.8.cloned.1.call-update) | async-done | bytes 6291472 | tf_op jit(solution)/shard_map/all_gather | solution.py:147
  221.2 7.9 %fusion.19 = f32[1536,448]{0,1:T(8,128)} fusion(bf16[1536,2048]{1,0:T(8,128)(2,1)} %all-gather.8.cloned.1.call-done, bf16[1,2048,448]{1,2,0:T(8,128)(2,1)} %param.23), kind=kOutput, calls=%fused_computation.30 | convolution fusion | flops 2818572288 | bytes 10878976 | tf_op jit(solution)/shard_map/dot_general | solution.py:148
  229.1 13.2 %convolution_convert_fusion = bf16[1536,2048]{1,0:T(8,128)(2,1)} fusion(bf16[1,448,2048]{2,1,0:T(8,128)(2,1)S(1)} %copy-done, bf16[1536,2048]{1,0:T(8,128)(2,1)} %all-gather.8.cloned.1.call-done, f32[1536,448]{0,1:T(8,128)} %fusion.19, bf16[1,2048,448]{1,2,0:T(8,128)(2,1)} %param.24), kind=kOutput, calls=%fused_computation.21 | convolution fusion | flops 5644419072 | bytes 19005440 | tf_op jit(solution)/shard_map/dot_general | solution.py:152
  242.3 65.9 %reduce-scatter.2.cloned.1.call-done = bf16[96,2048]{1,0:T(8,128)(2,1)} async-done(((bf16[1536,2048]{1,0:T(8,128)(2,1)}), bf16[96,2048]{1,0:T(8,128)(2,1)}) %reduce-scatter.2.cloned.1.call-update) | async-done | bytes 393232 | tf_op jit(solution)/shard_map/reduce_scatter | solution.py:151
  308.2 1.9 reshape.147
  310.2 7.2 %all-to-all-start.3 = ((bf16[16,6,2048]{2,1,0:T(8,128)(2,1)}), bf16[16,6,2048]{2,1,0:T(8,128)(2,1)S(1)}, u32[]{:S(2)}, u32[]{:S(2)}) async-start(bf16[16,6,2048]{2,1,0:T(8,128)(2,1)} %reshape.147), calls=%async_computation.4 | async-start | bytes 1048576 | tf_op jit(solution)/shard_map/all_to_all | solution.py:158
  317.7 8.5 %all-to-all-done.3 = bf16[16,6,2048]{2,1,0:T(8,128)(2,1)S(1)} async-done(((bf16[16,6,2048]{2,1,0:T(8,128)(2,1)}), bf16[16,6,2048]{2,1,0:T(8,128)(2,1)S(1)}, u32[]{:S(2)}, u32[]{:S(2)}) %all-to-all-start.3) | async-done | bytes 393248 | tf_op jit(solution)/shard_map/all_to_all | solution.py:158
  326.3 0.7 gather_fusion
  327.4 0.7 multiply_reduce_fusion
  (76 shorter events, 8.5 us)
Async XLA Ops:
  6.5 222.6 %copy-start = (bf16[1,448,2048]{2,1,0:T(8,128)(2,1)S(1)}, bf16[1,448,2048]{2,1,0:T(8,128)(2,1)}, u32[]{:S(2)}) copy-start(bf16[1,448,2048]{2,1,0:T(8,128)(2,1)} %param.25) | copy-start | bytes 5505028
  6.5 62.6 %all-gather.4.cloned.1.call-start = ((), (), s32[]{:S(2)}) async-start(), calls=%async_computation.5 | async-start | bytes 4456448 | tf_op jit(solution)/shard_map/all_gather | solution.py:31
  8.4 121.0 %all-gather.6.cloned.1.call-start = ((), (), s32[]{:S(2)}) async-start(), calls=%async_computation.6 | async-start | bytes 8912896 | tf_op jit(solution)/shard_map/all_gather | solution.py:124
  10.5 70.9 %all-to-all-start = ((f32[16,512,2]{1,2,0:T(2,128)}), f32[16,512,2]{1,2,0:T(2,128)S(1)}, u32[]{:S(2)}, u32[]{:S(2)}) async-start(f32[16,512,2]{1,2,0:T(2,128)} %broadcast_in_dim.61), calls=%async_computation | async-start | bytes 131072 | tf_op jit(solution)/shard_map/all_to_all | solution.py:12
  73.6 7.9 %copy-start.1 = (f32[512,2]{0,1:T(2,128)S(1)}, f32[512,2]{0,1:T(2,128)}, u32[]{:S(2)}) copy-start(f32[512,2]{0,1:T(2,128)} %param.20) | copy-start | bytes 12292
  81.5 47.9 %copy-start.2 = (bf16[32,2048]{1,0:T(8,128)(2,1)S(1)}, bf16[32,2048]{1,0:T(8,128)(2,1)}, u32[]{:S(2)}) copy-start(bf16[32,2048]{1,0:T(8,128)(2,1)} %param.16) | copy-start | bytes 393220
  99.0 17.7 %all-to-all-start.1 = ((bf16[16,32,128]{2,1,0:T(8,128)(2,1)}), bf16[16,32,128]{2,1,0:T(8,128)(2,1)S(1)}, u32[]{:S(2)}, u32[]{:S(2)}) async-start(bf16[16,32,128]{2,1,0:T(8,128)(2,1)} %all_to_all.24), calls=%async_computation.1 | async-start | bytes 262144 | tf_op jit(solution)/shard_map/all_to_all | solution.py:121
  106.1 115.1 %all-gather.8.cloned.1.call-start = ((), (), s32[]{:S(2)}) async-start(), calls=%async_computation.7 | async-start | bytes 6684672 | tf_op jit(solution)/shard_map/all_gather | solution.py:147
  106.4 28.1 %copy-start.3 = (f32[2048]{0:T(1024)S(1)}, f32[2048]{0:T(1024)}, u32[]{:S(2)}) copy-start(f32[2048]{0:T(1024)} %param.22) | copy-start | bytes 24580
  181.1 127.2 %reduce-scatter.2.cloned.1.call-start = ((), (), s32[]{:S(2)}) async-start(), calls=%async_computation.8 | async-start | bytes 6684672 | tf_op jit(solution)/shard_map/reduce_scatter | solution.py:151
  242.3 75.1 %copy-start.4 = (s32[32,2]{0,1:T(2,128)S(1)}, s32[32,2]{0,1:T(2,128)}, u32[]{:S(2)}) copy-start(s32[32,2]{0,1:T(2,128)} %param.26) | copy-start | bytes 772
  242.3 75.3 %copy-start.5 = (f32[32,2]{0,1:T(2,128)S(1)}, f32[32,2]{0,1:T(2,128)}, u32[]{:S(2)}) copy-start(f32[32,2]{0,1:T(2,128)} %param.27) | copy-start | bytes 772
  310.2 16.0 %all-to-all-start.3 = ((bf16[16,6,2048]{2,1,0:T(8,128)(2,1)}), bf16[16,6,2048]{2,1,0:T(8,128)(2,1)S(1)}, u32[]{:S(2)}, u32[]{:S(2)}) async-start(bf16[16,6,2048]{2,1,0:T(8,128)(2,1)} %reshape.147), calls=%async_computation.4 | async-start | bytes 1048576 | tf_op jit(solution)/shard_map/all_to_all | solution.py:158
Sparse Core Ops, SparseCore 0:
  9.8 59.3 all-gather.3
  71.0 58.3 all-gather.5
  181.2 40.0 all-gather.7
  242.5 65.7 reduce-scatter.1
where the time goes:
time: 336 us; the launch traced here: 335 us
  waiting for transfers between devices  187 us (56%)
  blocking collectives  44.9 us (13%)
  matrix products  29.4 us (9%)
  local copies, waits for them, and re-layouts  27.1 us (8%)
  starting transfers between devices  22.1 us (7%)
  between operations  13.3 us (4%)
  loops' own time  5.68 us (2%)
  other arithmetic  5.62 us (2%)
    reduce_scatter x1, waiting for transfers between devices, shards(): lax.psum_scatter(jnp.dot(hidden, down_weight[0], preferred_element_type=j...  65.9 us
    all_gather x1, waiting for transfers between devices, sent_together(): filled = lax.all_gather(both, axis, axis=dim, tiled=True)  49.1 us
    all_to_all x1, blocking collectives, shards(): lax.all_to_all(dispatch, 'sp', split_axis=0, concat_axis=0, tiled=True)  44.9 us
    all_gather x1, waiting for transfers between devices, shards(): rows_in = lax.all_gather(row_block, 'tp', axis=0, tiled=True)  40 us
    dot_general x1, matrix products, shards(): jnp.dot(hidden, down_weight[0], preferred_element_type=jnp.float32)  13.2 us
    all_gather x1, waiting for transfers between devices, shards(): lax.all_gather(out_weight, 'tp', axis=0, tiled=True)  12.6 us
    all_to_all x1, waiting for transfers between devices, shards(): lax.all_to_all(attended, 'tp', split_axis=0, concat_axis=1, tiled=True)  10.4 us
    unnamed x17, local copies, waits for them, and re-layouts  9.73 us
  transfers between devices with their start and end apart: 7, of which 6 were waited for; matrix products, arithmetic and copies ran while one was open for 8% of the time, Pallas kernels for 0%

commit v1 on v0

--- a/solution.py
+++ b/solution.py
@@ -144,7 +144,10 @@
     dispatch = dispatch.reshape(n_experts, capacity, model_width)
     arrived = lax.all_to_all(dispatch, "sp", split_axis=0, concat_axis=0, tiled=True)
     row_block = arrived.reshape(-1, model_width)
-    rows_in = lax.all_gather(row_block, "tp", axis=0, tiled=True)
+    peers_2 = lax.axis_size("tp")
+    blocks = jnp.stack([row_block for _ in range(peers_2)])
+    blocks = lax.all_to_all(blocks, "tp", split_axis=0, concat_axis=0)
+    rows_in = jnp.concatenate(blocks, axis=0)
     gate_value = jnp.dot(rows_in, gate_weight[0], preferred_element_type=jnp.float32)
     up_value = jnp.dot(rows_in, up_weight[0], preferred_element_type=jnp.float32)
     hidden = (jax.nn.silu(gate_value) * up_value).astype(jnp.bfloat16)

time: 336 us -> 435 us (1.29)
  blocking collectives: 44.9 us -> 187 us
  waiting for transfers between devices: 187 us -> 144 us
    all_to_all x0 -> x1, blocking collectives: none -> 142 us  [shards(): blocks = lax.all_to_all(blocks, 'tp', split_axis=0, concat_axis=0)]
    all_gather x1 -> x0, waiting for transfers between devices: 40 us -> none  [shards(): rows_in = lax.all_gather(row_block, 'tp', axis=0, tiled=True)]
    unnamed x17 -> x21, local copies, waits for them, and re-layouts: 9.73 us -> 12.4 us
  transfers between devices with their start and end apart: 7 -> 6, of which waited for: 6 -> 5; matrix products, arithmetic and copies ran while one was open for 8% -> 6% of each run, Pallas kernels for 0% -> 0%
where the time goes in v1:
time: 435 us; the launch traced here: 434 us
  blocking collectives  187 us (43%)
  waiting for transfers between devices  144 us (33%)
  local copies, waits for them, and re-layouts  29.7 us (7%)
  matrix products  26.1 us (6%)
  starting transfers between devices  21.8 us (5%)
  between operations  13.3 us (3%)
  loops' own time  5.68 us (1%)
  other arithmetic  5.62 us (1%)
    all_to_all x1, blocking collectives, shards(): blocks = lax.all_to_all(blocks, 'tp', split_axis=0, concat_axis=0)  142 us
    reduce_scatter x1, waiting for transfers between devices, shards(): lax.psum_scatter(jnp.dot(hidden, down_weight[0], preferred_element_type=j...  63.1 us
    all_gather x1, waiting for transfers between devices, sent_together(): filled = lax.all_gather(both, axis, axis=dim, tiled=True)  49.1 us
    all_to_all x1, blocking collectives, shards(): lax.all_to_all(dispatch, 'sp', split_axis=0, concat_axis=0, tiled=True)  44.9 us
    dot_general x1, matrix products, shards(): jnp.dot(hidden, down_weight[0], preferred_element_type=jnp.float32)  13.2 us
    all_gather x1, waiting for transfers between devices, shards(): lax.all_gather(out_weight, 'tp', axis=0, tiled=True)  12.6 us
    unnamed x21, local copies, waits for them, and re-layouts  12.4 us
    all_to_all x1, waiting for transfers between devices, shards(): lax.all_to_all(attended, 'tp', split_axis=0, concat_axis=1, tiled=True)  10.4 us
  transfers between devices with their start and end apart: 6, of which 5 were waited for; matrix products, arithmetic and copies ran while one was open for 6% of the time, Pallas kernels for 0%

profile of v1, /device:TPU:2, one launch (start us, length us, event | category | flops | bytes accessed | tf_op | source)
XLA Modules:
  0.0 433.9 jit_solution(18144878411443872926)
XLA Ops:
  6.5 1.8 pad_maximum_fusion
  9.2 1.3 broadcast_in_dim.61
  10.5 7.5 %all-to-all-start = ((f32[16,512,2]{1,2,0:T(2,128)}), f32[16,512,2]{1,2,0:T(2,128)S(1)}, u32[]{:S(2)}, u32[]{:S(2)}) async-start(f32[16,512,2]{1,2,0:T(2,128)} %broadcast_in_dim.61), calls=%async_computation | async-start | bytes 131072 | tf_op jit(solution)/shard_map/all_to_all | solution.py:12
  18.0 1.0 copy.28
  19.0 0.8 copy.33
  20.0 49.1 %all-gather.3.cloned.1.call-done = bf16[8192,256]{1,0:T(8,128)(2,1)} async-done(((bf16[512,256]{1,0:T(8,128)(2,1)}), bf16[8192,256]{1,0:T(8,128)(2,1)}) %all-gather.3.cloned.1.call-update) | async-done | bytes 4194320 | tf_op jit(solution)/shard_map/all_gather | solution.py:31
  69.2 4.4 %fusion.30 = (bf16[8192,128]{1,0:T(8,128)(2,1)}, bf16[8192,128]{1,0:T(8,128)(2,1)}) fusion(bf16[8192,256]{1,0:T(8,128)(2,1)} %all-gather.3.cloned.1.call-done), kind=kLoop, calls=%fused_computation.54 | loop fusion | bytes 8388608 | tf_op jit(solution)/shard_map/split | solution.py:32
  73.6 3.9 copy.29
  77.5 3.9 copy.30
  81.5 16.5 %while.15 = (s32[]{:T(128)}, f32[2,512]{1,0:T(2,128)S(1)}, f32[2,512]{1,0:T(2,128)S(1)}, f32[2,512,64]{1,2,0:T(8,128)S(1)}, s32[8]{0:T(128)S(1)}, /*index=5*/s32...) while((s32[]{:T(128)}, f32[2,512]{1,0:T(2,128)S(1)}, ...), condition=%wide.region_5.6_spmd.clone, body=%wide.region_0.5_spmd.clone.sunk | while | flops 289017344 | bytes 17043828 | solution.py:113
  82.8 6.2 %conditional.3 = ((f32[2,512]{1,0:T(2,128)S(1)}, f32[2,512]{1,0:T(2,128)S(1)}, f32[2,512,64]{1,2,0:T(8,128)S(1)})) conditional(s32[]{:T(128)} %convert_element_type.83, (f32[2,512]{1,0:T(2,128)S(1)}, f32[2,512]{1,0:T(2,128)S(1)}, f32[2,512,64]{1,2,0:T(8,128)S(1)}) %tuple.43, (s32[]{:T(128)}, s32[]{:T(128)}, bf16[8,1024,128]{1,2,0:T(8,128)(2,1)}, ...), branch_computations={%region_1.1_spmd, %region_2.4_spmd} | conditional | flops 289017344 | bytes 17041490 | solution.py:111
  83.3 1.1 constant_dynamic-slice_fusion
  84.3 1.4 fusion.4
  85.7 1.5 fusion.3
  87.2 1.7 fusion.8
  98.2 0.8 all_to_all.27
  99.0 7.1 %all-to-all-start.1 = ((bf16[16,32,128]{2,1,0:T(8,128)(2,1)}), bf16[16,32,128]{2,1,0:T(8,128)(2,1)S(1)}, u32[]{:S(2)}, u32[]{:S(2)}) async-start(bf16[16,32,128]{2,1,0:T(8,128)(2,1)} %all_to_all.27), calls=%async_computation.1 | async-start | bytes 262144 | tf_op jit(solution)/shard_map/all_to_all | solution.py:121
  106.4 10.4 %all-to-all-done.1 = bf16[16,32,128]{2,1,0:T(8,128)(2,1)S(1)} async-done(((bf16[16,32,128]{2,1,0:T(8,128)(2,1)}), bf16[16,32,128]{2,1,0:T(8,128)(2,1)S(1)}, u32[]{:S(2)}, u32[]{:S(2)}) %all-to-all-start.1) | async-done | bytes 131104 | tf_op jit(solution)/shard_map/all_to_all | solution.py:121
  116.8 12.6 %all-gather.5.cloned.1.call-done = bf16[2048,2048]{1,0:T(8,128)(2,1)} async-done(((bf16[128,2048]{1,0:T(8,128)(2,1)}), bf16[2048,2048]{1,0:T(8,128)(2,1)}) %all-gather.5.cloned.1.call-update) | async-done | bytes 8388624 | tf_op jit(solution)/shard_map/all_gather | solution.py:124
  129.4 5.0 %multiply_reduce_fusion.1 = (f32[32]{0:T(128)S(1)}, f32[32,2048]{1,0:T(8,128)S(1)}) fusion(bf16[2048,2048]{1,0:T(8,128)(2,1)} %all-gather.5.cloned.1.call-done, bf16[32,2048]{1,0:T(8,128)(2,1)S(1)} %copy-done.3, bf16[16,32,128]{2,1,0:T(8,128)(2,1)S(1)} %all-to-all-done.1), kind=kOutput, calls=%fused_computation.36 | convolution fusion | flops 268828640 | bytes 8913024 | tf_op jit(solution)/shard_map/dot_general | solution.py:122
  135.2 44.9 %all_to_all.39 = bf16[16,6,2048]{2,1,0:T(8,128)(2,1)S(1)} all-to-all(bf16[16,6,2048]{2,1,0:T(8,128)(2,1)S(1)} %reshape.147), channel_id=1, replica_groups=mesh['sp'=16,'tp'=16] {'sp'}, dimensions={0} | all-to-all | bytes 786432 | tf_op jit(solution)/shard_map/all_to_all | solution.py:145
  180.2 0.8 stack.3
  181.1 142.3 %all_to_all.40 = bf16[16,96,2048]{2,1,0:T(8,128)(2,1)S(1)} all-to-all(bf16[16,96,2048]{2,1,0:T(8,128)(2,1)S(1)} %stack.3), channel_id=1, replica_groups=mesh['sp'=16,'tp'=16] {'tp'}, dimensions={0} | all-to-all | bytes 12582912 | tf_op jit(solution)/shard_map/all_to_all | solution.py:149
  323.4 2.7 copy-done.1
  326.0 4.6 %fusion.19 = f32[1536,448]{0,1:T(8,128)} fusion(bf16[1536,2048]{1,0:T(8,128)(2,1)S(1)} %bitcast.64, bf16[1,2048,448]{1,2,0:T(8,128)(2,1)S(1)} %copy-done.7), kind=kOutput, calls=%fused_computation.30 | convolution fusion | flops 2818572288 | bytes 10878976 | tf_op jit(solution)/shard_map/dot_general | solution.py:151
  330.6 13.2 %convolution_convert_fusion = bf16[1536,2048]{1,0:T(8,128)(2,1)} fusion(bf16[1,448,2048]{2,1,0:T(8,128)(2,1)S(1)} %copy-done, bf16[1536,2048]{1,0:T(8,128)(2,1)} %bitcast.65, f32[1536,448]{0,1:T(8,128)} %fusion.19, bf16[1,2048,448]{1,2,0:T(8,128)(2,1)} %param.24), kind=kOutput, calls=%fused_computation.21 | convolution fusion | flops 5644419072 | bytes 19005440 | tf_op jit(solution)/shard_map/dot_general | solution.py:155
  343.9 63.1 %reduce-scatter.2.cloned.1.call-done = bf16[96,2048]{1,0:T(8,128)(2,1)} async-done(((bf16[1536,2048]{1,0:T(8,128)(2,1)}), bf16[96,2048]{1,0:T(8,128)(2,1)}) %reduce-scatter.2.cloned.1.call-update) | async-done | bytes 393232 | tf_op jit(solution)/shard_map/reduce_scatter | solution.py:154
  406.9 1.9 reshape.149
  408.8 7.1 %all-to-all-start.4 = ((bf16[16,6,2048]{2,1,0:T(8,128)(2,1)}), bf16[16,6,2048]{2,1,0:T(8,128)(2,1)S(1)}, u32[]{:S(2)}, u32[]{:S(2)}) async-start(bf16[16,6,2048]{2,1,0:T(8,128)(2,1)} %reshape.149), calls=%async_computation.5 | async-start | bytes 1048576 | tf_op jit(solution)/shard_map/all_to_all | solution.py:161
  416.3 8.5 %all-to-all-done.4 = bf16[16,6,2048]{2,1,0:T(8,128)(2,1)S(1)} async-done(((bf16[16,6,2048]{2,1,0:T(8,128)(2,1)}), bf16[16,6,2048]{2,1,0:T(8,128)(2,1)S(1)}, u32[]{:S(2)}, u32[]{:S(2)}) %all-to-all-start.4) | async-done | bytes 393248 | tf_op jit(solution)/shard_map/all_to_all | solution.py:161
  424.9 0.7 gather_fusion
  425.9 0.7 multiply_reduce_fusion
  (79 shorter events, 9.1 us)
Async XLA Ops:
  6.5 324.1 %copy-start = (bf16[1,448,2048]{2,1,0:T(8,128)(2,1)S(1)}, bf16[1,448,2048]{2,1,0:T(8,128)(2,1)}, u32[]{:S(2)}) copy-start(bf16[1,448,2048]{2,1,0:T(8,128)(2,1)} %param.25) | copy-start | bytes 5505028
  6.5 62.6 %all-gather.3.cloned.1.call-start = ((), (), s32[]{:S(2)}) async-start(), calls=%async_computation.6 | async-start | bytes 4456448 | tf_op jit(solution)/shard_map/all_gather | solution.py:31
  8.4 121.0 %all-gather.5.cloned.1.call-start = ((), (), s32[]{:S(2)}) async-start(), calls=%async_computation.7 | async-start | bytes 8912896 | tf_op jit(solution)/shard_map/all_gather | solution.py:124
  10.5 70.9 %all-to-all-start = ((f32[16,512,2]{1,2,0:T(2,128)}), f32[16,512,2]{1,2,0:T(2,128)S(1)}, u32[]{:S(2)}, u32[]{:S(2)}) async-start(f32[16,512,2]{1,2,0:T(2,128)} %broadcast_in_dim.61), calls=%async_computation | async-start | bytes 131072 | tf_op jit(solution)/shard_map/all_to_all | solution.py:12
  73.6 7.9 %copy-start.2 = (f32[512,2]{0,1:T(2,128)S(1)}, f32[512,2]{0,1:T(2,128)}, u32[]{:S(2)}) copy-start(f32[512,2]{0,1:T(2,128)} %param.20) | copy-start | bytes 12292
  81.5 47.9 %copy-start.3 = (bf16[32,2048]{1,0:T(8,128)(2,1)S(1)}, bf16[32,2048]{1,0:T(8,128)(2,1)}, u32[]{:S(2)}) copy-start(bf16[32,2048]{1,0:T(8,128)(2,1)} %param.16) | copy-start | bytes 393220
  99.0 17.8 %all-to-all-start.1 = ((bf16[16,32,128]{2,1,0:T(8,128)(2,1)}), bf16[16,32,128]{2,1,0:T(8,128)(2,1)S(1)}, u32[]{:S(2)}, u32[]{:S(2)}) async-start(bf16[16,32,128]{2,1,0:T(8,128)(2,1)} %all_to_all.27), calls=%async_computation.1 | async-start | bytes 262144 | tf_op jit(solution)/shard_map/all_to_all | solution.py:121
  106.1 300.8 %reduce-scatter.2.cloned.1.call-start = ((), (), s32[]{:S(2)}) async-start(), calls=%async_computation.8 | async-start | bytes 6684672 | tf_op jit(solution)/shard_map/reduce_scatter | solution.py:154
  106.4 28.1 %copy-start.4 = (f32[2048]{0:T(1024)S(1)}, f32[2048]{0:T(1024)}, u32[]{:S(2)}) copy-start(f32[2048]{0:T(1024)} %param.22) | copy-start | bytes 24580
  181.1 145.0 %copy-start.7 = (bf16[1,2048,448]{1,2,0:T(8,128)(2,1)S(1)}, bf16[1,2048,448]{1,2,0:T(8,128)(2,1)}, u32[]{:S(2)}) copy-start(bf16[1,2048,448]{1,2,0:T(8,128)(2,1)} %param.23) | copy-start | bytes 5505028
  323.4 2.7 copy-start.1
  343.8 72.1 %copy-start.5 = (s32[32,2]{0,1:T(2,128)S(1)}, s32[32,2]{0,1:T(2,128)}, u32[]{:S(2)}) copy-start(s32[32,2]{0,1:T(2,128)} %param.26) | copy-start | bytes 772
  343.8 72.3 %copy-start.6 = (f32[32,2]{0,1:T(2,128)S(1)}, f32[32,2]{0,1:T(2,128)}, u32[]{:S(2)}) copy-start(f32[32,2]{0,1:T(2,128)} %param.27) | copy-start | bytes 772
  408.8 15.9 %all-to-all-start.4 = ((bf16[16,6,2048]{2,1,0:T(8,128)(2,1)}), bf16[16,6,2048]{2,1,0:T(8,128)(2,1)S(1)}, u32[]{:S(2)}, u32[]{:S(2)}) async-start(bf16[16,6,2048]{2,1,0:T(8,128)(2,1)} %reshape.149), calls=%async_computation.5 | async-start | bytes 1048576 | tf_op jit(solution)/shard_map/all_to_all | solution.py:161
Sparse Core Ops, SparseCore 0:
  9.8 59.3 all-gather.2
  71.0 58.3 all-gather.4
  344.0 62.9 reduce-scatter.1
